TPU v7x, 256 devices: a 2x2x32 block of a 4x16x32 slice. The times are simulated.
256 devices in a mesh: grp: 4 (over y, x), ep: 32 (over z), tp: 2 (over core).
Axes of the slice: x: 2, y: 2, z: 32, core: 2. Of those that a mesh axis runs over, the one named last changes fastest.
The devices are a block of a 4x16x32 slice.
Arguments:
- tokens: bfloat16 [65536, 2048], P(('grp', 'ep', 'tp')), parts along dimension 0, may hold values from -6 to 6
- norm_gain: float32 [2048], replicated, may hold values from 0.1 to 1.9
- route_ids: int32 [65536, 2], P(('grp', 'ep', 'tp')), parts along dimension 0, may hold values from 0 to 31, as said below
- route_weights: float32 [65536, 2], P(('grp', 'ep', 'tp')), parts along dimension 0, may hold values from 0.1 to 1
- w_gate: bfloat16 [32, 2048, 512], P('ep', None, 'tp'), may hold values from -0.125 to 0.125
- w_up: bfloat16 [32, 2048, 512], P('ep', None, 'tp'), may hold values from -0.125 to 0.125
- w_down: bfloat16 [32, 512, 2048], P('ep', 'tp'), may hold values from -0.25 to 0.25
Outputs:
- mixed: bfloat16 [65536, 2048], P(('grp', 'ep', 'tp')), parts along dimension 0
There are 4 independent parts, one for each index of `grp`. A program takes and returns all parts, laid end to end along the dimension named above; an argument that names none is the same for every part. Nothing has to cross between parts.
Inputs may be any that keep to these rules, and one draw needn't show every extreme that they name: `route_ids`: the 2 experts of a token are different and lie in one group of 8 consecutive experts. Among the tokens of one device (aligned blocks of 256 tokens) no expert is named more than 32 times, and in every such block some expert is named exactly 32 times.
All inputs are finite; a program needn't handle non-finite values.
Results may differ from a plain program's by a relative error of at most 0.007.
Values may be sent and summed in bfloat16 or wider, within the bound.
A program may use at most 128 MiB of HBM per device.

v0:
```python
import jax
import jax.numpy as jnp
from jax import lax
from jax.sharding import PartitionSpec as P

GROUPS = 4


epsilon = 1e-06


def send_back(result):
    return lax.all_to_all(result, "ep", split_axis=0, concat_axis=0, tiled=True)


def per_device(tokens, norm_gain, route_ids, route_weights, w_gate, w_up, w_down):
    row_count, features = tokens.shape
    top_count = route_ids.shape[1]
    local_experts = w_gate.shape[0]
    ep_size = lax.axis_size("ep")
    experts_all = ep_size * local_experts
    capacity = row_count * GROUPS // experts_all
    floats = tokens.astype(jnp.float32)
    inverse = lax.rsqrt(jnp.mean(floats * floats, axis=1, keepdims=True) + epsilon)
    normed = (floats * inverse * norm_gain).astype(jnp.bfloat16)
    flat_ids = route_ids.reshape(-1)
    onehot = (flat_ids[:, None] == jnp.arange(experts_all, dtype=jnp.int32)[None, :]).astype(
        jnp.int32
    )
    earlier = jnp.cumsum(onehot, axis=0) - onehot
    slot_index = jnp.sum(earlier * onehot, axis=1)
    target = (flat_ids * capacity + slot_index).reshape(row_count, top_count)
    outbound = jnp.zeros((experts_all * capacity, features), jnp.bfloat16)
    for column in range(top_count):
        outbound = outbound.at[target[:, column]].set(normed)
    outbound = outbound.reshape(ep_size, local_experts, capacity, features)
    full_gate, full_up, full_down = (
        lax.all_gather(w_gate, "tp", axis=2, tiled=True),
        lax.all_gather(w_up, "tp", axis=2, tiled=True),
        lax.all_gather(w_down, "tp", axis=1, tiled=True),
    )
    arrived = lax.all_to_all(outbound, "ep", split_axis=0, concat_axis=0, tiled=True)
    gate_pre = jnp.einsum("sjcd,jdf->sjcf", arrived, full_gate, preferred_element_type=jnp.float32)
    up_pre = jnp.einsum("sjcd,jdf->sjcf", arrived, full_up, preferred_element_type=jnp.float32)
    hidden = (jax.nn.silu(gate_pre) * up_pre).astype(jnp.bfloat16)
    result = jnp.einsum("sjcf,jfd->sjcd", hidden, full_down, preferred_element_type=jnp.float32)
    returned_rows = send_back(result.astype(jnp.bfloat16))
    returned_rows = returned_rows.reshape(experts_all * capacity, features)
    combined = jnp.zeros((row_count, features), jnp.float32)
    for column in range(top_count):
        picked = returned_rows[target[:, column]].astype(jnp.float32)
        combined = combined + route_weights[:, column : column + 1] * picked
    return combined.astype(jnp.bfloat16)


def solution(mesh):
    in_specs = (
        P(("grp", "ep", "tp"), None),
        P(),
        P(("grp", "ep", "tp"), None),
        P(("grp", "ep", "tp"), None),
        P("ep", None, "tp"),
        P("ep", None, "tp"),
        P("ep", "tp", None),
    )
    out_specs = P(("grp", "ep", "tp"), None)
    return jax.shard_map(
        per_device, mesh=mesh, in_specs=in_specs, out_specs=out_specs, check_vma=False
    )
```

profile of v0, /device:TPU:46, one launch (start us, length us, event | category | flops | bytes accessed | tf_op | source)
XLA Modules:
  0.0 835.7 jit_solution(127563947804727679)
XLA Ops:
  6.5 0.0 copy-start
  6.5 0.0 copy-start.1
  6.6 0.9 copy.25
  7.5 0.1 eq.29
  7.6 0.1 eq.25
  7.8 1.2 reduce-window.6
  8.9 0.2 slice_reduce_fusion
  9.2 0.1 fusion.35
  9.3 0.1 reduce_sum.21
  9.5 0.1 copy.28
  9.5 0.7 multiply_add_fusion
  10.2 1.5 fusion.4
  11.8 0.0 copy-done
  11.8 0.0 copy-done.1
  11.8 5.0 scatter_custom_fusion
  16.8 7.2 scatter_custom_fusion.1
  23.9 32.7 %all-to-all-start = ((bf16[32,1,32,2048]{3,2,1,0:T(8,128)(2,1)}), bf16[32,1,32,2048]{3,2,1,0:T(8,128)(2,1)}, u32[]{:S(2)}, u32[]{:S(2)}) async-start(bf16[32,1,32,2048]{3,2,1,0:T(8,128)(2,1)} %bitcast.101), calls=%async_computation | async-start | bytes 8388608 | tf_op jit(solution)/shard_map/all_to_all | solution.py:42
  56.6 0.1 all-gather.4.cloned.1.call-start
  56.7 0.7 all-gather.4.cloned.1.call-update
  57.4 0.1 all-gather.6.cloned.1.call-start
  57.5 0.7 all-gather.6.cloned.1.call-update
  58.2 0.2 all-gather.8.cloned.1.call-start
  58.5 0.5 all-gather.8.cloned.1.call-update
  59.0 27.9 %all-gather.4.cloned.1.call-done = bf16[1,2048,512]{2,1,0:T(8,128)(2,1)} async-done(((bf16[1,2048,256]{2,1,0:T(8,128)(2,1)}), bf16[1,2048,512]{2,1,0:T(8,128)(2,1)}) %all-gather.4.cloned.1.call-update) | async-done | bytes 2097168 | tf_op jit(solution)/shard_map/all_gather | solution.py:38
  86.9 330.7 %all-to-all-done = bf16[32,1,32,2048]{3,2,1,0:T(8,128)(2,1)} async-done(((bf16[32,1,32,2048]{3,2,1,0:T(8,128)(2,1)}), bf16[32,1,32,2048]{3,2,1,0:T(8,128)(2,1)}, u32[]{:S(2)}, u32[]{:S(2)}) %all-to-all-start) | async-done | bytes 4194336 | tf_op jit(solution)/shard_map/all_to_all | solution.py:42
  417.6 5.2 fusion.2
  422.8 0.0 all-gather.6.cloned.1.call-done
  422.9 0.0 all-gather.8.cloned.1.call-done
  422.9 10.1 %convert_bitcast_fusion = bf16[32,1,32,2048]{3,2,1,0:T(8,128)(2,1)} fusion(bf16[1,512,2048]{2,1,0:T(8,128)(2,1)} %all-gather.8.cloned.1.call-done, bf16[1,2048,512]{2,1,0:T(8,128)(2,1)} %all-gather.6.cloned.1.call-done, bf16[32,1,32,2048]{3,2,1,0:T(8,128)(2,1)} %all-to-all-done, f32[32,32,512]{2,1,0:T(8,128)S(1)} %fusion.2), kind=kOutput, calls=%fused_computation.8 | convolution fusion | flops 4300210176 | bytes 14680064 | tf_op jit(solution)/shard_map/sjcf,jfd->sjcd/dot_general | solution.py:46
  432.9 0.0 copy-start.2
  432.9 22.0 %all-to-all-start.1 = ((bf16[32,1,32,2048]{3,2,1,0:T(8,128)(2,1)}), bf16[32,1,32,2048]{3,2,1,0:T(8,128)(2,1)}, u32[]{:S(2)}, u32[]{:S(2)}) async-start(bf16[32,1,32,2048]{3,2,1,0:T(8,128)(2,1)} %convert_bitcast_fusion), calls=%async_computation.1 | async-start | bytes 8388608 | tf_op jit(solution)/shard_map/all_to_all | solution.py:13
  454.9 0.0 copy-done.2
  455.0 362.6 %all-to-all-done.1 = bf16[32,1,32,2048]{3,2,1,0:T(8,128)(2,1)} async-done(((bf16[32,1,32,2048]{3,2,1,0:T(8,128)(2,1)}), bf16[32,1,32,2048]{3,2,1,0:T(8,128)(2,1)}, u32[]{:S(2)}, u32[]{:S(2)}) %all-to-all-start.1) | async-done | bytes 4194336 | tf_op jit(solution)/shard_map/all_to_all | solution.py:13
  817.5 5.1 gather_fusion
  822.6 5.1 gather_fusion.1
  827.7 1.4 add_convert_fusion
  (8 shorter events, 0.1 us)
Async XLA Ops:
  6.5 5.2 copy-start
  6.5 5.2 copy-start.1
  23.9 393.7 %all-to-all-start = ((bf16[32,1,32,2048]{3,2,1,0:T(8,128)(2,1)}), bf16[32,1,32,2048]{3,2,1,0:T(8,128)(2,1)}, u32[]{:S(2)}, u32[]{:S(2)}) async-start(bf16[32,1,32,2048]{3,2,1,0:T(8,128)(2,1)} %bitcast.101), calls=%async_computation | async-start | bytes 8388608 | tf_op jit(solution)/shard_map/all_to_all | solution.py:42
  56.6 30.3 %all-gather.4.cloned.1.call-start = ((), (), s32[]{:S(2)}) async-start(), calls=%async_computation.2 | async-start | bytes 3145728 | tf_op jit(solution)/shard_map/all_gather | solution.py:38
  57.4 365.4 %all-gather.6.cloned.1.call-start = ((), (), s32[]{:S(2)}) async-start(), calls=%async_computation.3 | async-start | bytes 3145728 | tf_op jit(solution)/shard_map/all_gather | solution.py:39
  58.2 364.7 %all-gather.8.cloned.1.call-start = ((), (), s32[]{:S(2)}) async-start(), calls=%async_computation.4 | async-start | bytes 3145728 | tf_op jit(solution)/shard_map/all_gather | solution.py:40
  432.9 22.0 %copy-start.2 = (f32[256,2]{0,1:T(2,128)S(1)}, f32[256,2]{0,1:T(2,128)}, u32[]{:S(2)}) copy-start(f32[256,2]{0,1:T(2,128)} %param.10) | copy-start | bytes 6148
  432.9 384.6 %all-to-all-start.1 = ((bf16[32,1,32,2048]{3,2,1,0:T(8,128)(2,1)}), bf16[32,1,32,2048]{3,2,1,0:T(8,128)(2,1)}, u32[]{:S(2)}, u32[]{:S(2)}) async-start(bf16[32,1,32,2048]{3,2,1,0:T(8,128)(2,1)} %convert_bitcast_fusion), calls=%async_computation.1 | async-start | bytes 8388608 | tf_op jit(solution)/shard_map/all_to_all | solution.py:13
Sparse Core Ops, SparseCore 0:
  59.2 27.6 all-gather.3
  88.7 28.3 all-gather.5
  119.0 28.8 all-gather.7
where the time goes:
time: 849 us; the launch traced here: 836 us
  waiting for transfers between devices  723 us (85%)
  starting transfers between devices  55 us (6%)
  other arithmetic  17.1 us (2%)
  matrix products  15.2 us (2%)
  between operations  13.3 us (2%)
  local copies, waits for them, and re-layouts  11.8 us (1%)
    all_to_all x1, waiting for transfers between devices, send_back(): return lax.all_to_all(result, 'ep', split_axis=0, concat_axis=0, tiled=True)  363 us
    all_to_all x1, waiting for transfers between devices, per_device(): lax.all_to_all(outbound, 'ep', split_axis=0, concat_axis=0, tiled=True)  331 us
    all_to_all x1, starting transfers between devices, per_device(): lax.all_to_all(outbound, 'ep', split_axis=0, concat_axis=0, tiled=True)  32.7 us
    all_gather x1, waiting for transfers between devices, per_device(): lax.all_gather(w_gate, 'tp', axis=2, tiled=True)  27.9 us
    all_to_all x1, starting transfers between devices, send_back(): return lax.all_to_all(result, 'ep', split_axis=0, concat_axis=0, tiled=True)  22 us
  transfers between devices with their start and end apart: 5, of which 3 were waited for; matrix products, arithmetic and copies ran while one was open for 1% of the time, Pallas kernels for 0%

commit v1 on v0

v1 whole, which is shorter than its diff:
```python
import functools

import jax
import jax.numpy as jnp
from jax import lax
from jax.experimental import pallas as pl
from jax.experimental.pallas import tpu as pltpu
from jax.sharding import PartitionSpec as P

GROUPS = 4

epsilon = 1e-06

CHUNK = 16
LAG = 3
CHUNKS = 128
SLOTS = 4
LANES = 128


def send_back(result):
    return lax.all_to_all(result, "ep", split_axis=0, concat_axis=0, tiled=True)


def ring_setup():
    ep = lax.axis_size("ep")
    me = lax.axis_index("ep")
    up, down = lax.rem(me + 1, ep), lax.rem(me + ep - 1, ep)
    barrier = pltpu.get_barrier_semaphore()
    for peer in (up, down):
        pl.semaphore_signal(
            barrier, inc=1, device_id={"ep": peer}, device_id_type=pl.DeviceIdType.MESH
        )
    pl.semaphore_wait(barrier, 2)
    return up, down


def chunk_copy(send, land, send_sem, recv_sem, peer, way, slot, chunk):
    return pltpu.make_async_remote_copy(
        src_ref=send.at[way, slot],
        dst_ref=land.at[way, chunk],
        send_sem=send_sem.at[way, slot],
        recv_sem=recv_sem.at[way, chunk],
        device_id={"ep": peer},
        device_id_type=pl.DeviceIdType.MESH,
    )


def ring_stream(peers, order, build, keep, send, land, send_sem, recv_sem):
    def receive(step):
        for way in (0, 1):
            chunk = order(step)
            chunk_copy(send, land, send_sem, recv_sem, peers[way], way, 0, chunk).wait_recv()
            keep(way, chunk)

    def drain(step):
        slot = lax.rem(step, SLOTS)
        for way in (0, 1):
            chunk_copy(
                send, land, send_sem, recv_sem, peers[way], way, slot, order(step)
            ).wait_send()

    def body(step, carry):
        slot = lax.rem(step, SLOTS)

        @pl.when(step >= LAG)
        def _():
            receive(step - LAG)

        @pl.when(step >= SLOTS)
        def _():
            drain(step - SLOTS)

        for way in (0, 1):
            build(way, slot, order(step))
        for way in (0, 1):
            chunk_copy(
                send, land, send_sem, recv_sem, peers[way], way, slot, order(step)
            ).start()
        return carry

    lax.fori_loop(0, CHUNKS, body, 0)
    for step in range(CHUNKS - LAG, CHUNKS):
        receive(step)
    for step in range(CHUNKS - SLOTS, CHUNKS):
        drain(step)


def dispatch_kernel(
    pick_ref, expert_ref, own_ref, out_ref, store, send, land, send_sem, recv_sem
):
    rows = CHUNKS * CHUNK
    peers = ring_setup()
    own_rows = own_ref.shape[0]

    def take(block, carry):
        at = pl.multiple_of(block * CHUNK, CHUNK)
        store[pl.ds(2 * rows + at, CHUNK)] = own_ref[pl.ds(at, CHUNK)]
        return carry

    lax.fori_loop(0, own_rows // CHUNK, take, 0)
    store[pl.ds(2 * rows + own_rows, 1)] = jnp.zeros((1,) + own_ref.shape[1:], own_ref.dtype)

    def keep(way, chunk):
        store[pl.ds(way * rows + chunk * CHUNK, CHUNK)] = land[way, chunk]

    def build(way, slot, chunk):
        for row in range(CHUNK):
            send[way, slot, row] = store[pick_ref[way, chunk * CHUNK + row]]

    ring_stream(peers, lambda step: step, build, keep, send, land, send_sem, recv_sem)

    def gather(block, carry):
        for row in range(CHUNK):
            at = block * CHUNK + row
            out_ref[at] = store[expert_ref[at]]
        return carry

    lax.fori_loop(0, out_ref.shape[0] // CHUNK, gather, 0)


def collect_kernel(
    result_ref, onward_ref, final_ref, result, out_ref, store, send, land, send_sem, recv_sem
):
    rows = CHUNKS * CHUNK
    up, down = ring_setup()
    store[pl.ds(2 * rows, 1)] = jnp.zeros((1,) + store.shape[1:], store.dtype)

    def keep(way, chunk):
        store[pl.ds(way * rows + chunk * CHUNK, CHUNK)] = land[way, chunk]

    def build(way, slot, chunk):
        for row in range(CHUNK):
            at = chunk * CHUNK + row
            here = result[result_ref[way, at]].astype(jnp.float32)
            beyond = store[onward_ref[way, at]].astype(jnp.float32)
            send[way, slot, row] = (here + beyond).astype(send.dtype)

    ring_stream(
        (down, up),
        lambda step: CHUNKS - 1 - step,
        build,
        keep,
        send,
        land,
        send_sem,
        recv_sem,
    )

    def finish(block, carry):
        for row in range(CHUNK):
            at = block * CHUNK + row
            total = result[final_ref[2, at]].astype(jnp.float32)
            for way in (0, 1):
                total = total + store[final_ref[way, at]].astype(jnp.float32)
            out_ref[at] = total.astype(out_ref.dtype)
        return carry

    lax.fori_loop(0, out_ref.shape[0] // CHUNK, finish, 0)


def ring_call(kernel, name, collective_id, out_rows, store_rows, index_args, data):
    row_shape = data.shape[1:]
    smem = pl.BlockSpec(memory_space=pltpu.SMEM)
    vmem = pl.BlockSpec(memory_space=pltpu.VMEM)
    return pl.pallas_call(
        kernel,
        out_shape=jax.ShapeDtypeStruct((out_rows,) + row_shape, jnp.bfloat16),
        in_specs=[smem] * len(index_args) + [vmem],
        out_specs=vmem,
        scratch_shapes=[
            pltpu.VMEM((store_rows,) + row_shape, jnp.bfloat16),
            pltpu.VMEM((2, SLOTS, CHUNK) + row_shape, jnp.bfloat16),
            pltpu.VMEM((2, CHUNKS, CHUNK) + row_shape, jnp.bfloat16),
            pltpu.SemaphoreType.DMA((2, SLOTS)),
            pltpu.SemaphoreType.DMA((2, CHUNKS)),
        ],
        compiler_params=pltpu.CompilerParams(
            collective_id=collective_id,
            has_side_effects=True,
            vmem_limit_bytes=60 * 1024 * 1024,
        ),
        name=name,
    )(*index_args, data)


def dispatch(pick, expert, own):
    rows = CHUNKS * CHUNK
    return ring_call(
        dispatch_kernel,
        "dispatch",
        0,
        expert.shape[0],
        2 * rows + own.shape[0] + 1,
        (pick, expert),
        own,
    )


def collect(result_pick, onward, final, result):
    rows = CHUNKS * CHUNK
    return ring_call(
        collect_kernel,
        "collect",
        1,
        final.shape[1],
        2 * rows + 1,
        (result_pick, onward, final),
        result,
    )


def plan_routes(route_ids, route_weights, capacity):
    ep = lax.axis_size("ep")
    me = lax.axis_index("ep")
    tokens = route_ids.shape[0]
    steps = ep // 2 + ep // GROUPS
    low = jnp.min(route_ids, axis=1)
    high = jnp.max(route_ids, axis=1)
    ahead = jnp.maximum((low - me) % ep, (high - me) % ep)
    behind = jnp.maximum((me - low) % ep, (me - high) % ep)
    inside = (low <= me) & (me <= high)
    upward = ahead <= behind
    reach = jnp.stack(
        [
            jnp.where(inside, high - me, jnp.where(upward, ahead, 0)),
            jnp.where(inside, me - low, jnp.where(upward, 0, behind)),
        ]
    )
    position = jnp.arange(tokens, dtype=jnp.int32)
    before = position[None, :] < position[:, None]
    further = (reach[:, None, :] > reach[:, :, None]) | (
        (reach[:, None, :] == reach[:, :, None]) & before[None]
    )
    rank = jnp.sum(further.astype(jnp.int32), axis=2)
    alive = jnp.sum(
        (reach[:, :, None] > jnp.arange(steps, dtype=jnp.int32)[None, None, :]).astype(jnp.int32),
        axis=1,
    )
    same = jnp.zeros((tokens, route_ids.shape[1]), jnp.int32)
    for column in range(route_ids.shape[1]):
        match = route_ids[:, :, None] == route_ids[None, None, :, column].reshape(1, 1, tokens)
        same = same + jnp.sum((match & before[:, None, :]).astype(jnp.int32), axis=2)
    target = route_ids * capacity + same
    goes_up = jnp.where(inside[:, None], route_ids > me, upward[:, None])
    code = jnp.where(goes_up, rank[0][:, None], tokens + rank[1][:, None])
    code = jnp.where(route_ids == me, 2 * tokens + position[:, None], code)
    slots = jnp.arange(ep * capacity, dtype=jnp.int32)
    sent_code = jnp.zeros((ep * capacity,), jnp.float32)
    sent_weight = jnp.zeros((ep * capacity,), jnp.float32)
    for column in range(route_ids.shape[1]):
        hit = slots[:, None] == target[None, :, column]
        sent_code = sent_code + jnp.sum(
            jnp.where(hit, (code[:, column] + 1).astype(jnp.float32)[None, :], 0.0), axis=1
        )
        sent_weight = sent_weight + jnp.sum(
            jnp.where(hit, route_weights[:, column][None, :], 0.0), axis=1
        )
    counts = alive.astype(jnp.float32).reshape(1, 2 * steps)
    message = jnp.concatenate(
        [
            sent_code.reshape(ep, capacity),
            sent_weight.reshape(ep, capacity),
            jnp.broadcast_to(counts, (ep, 2 * steps)),
        ],
        axis=1,
    )
    message = jnp.pad(message, ((0, 0), (0, LANES - message.shape[1])))
    return message, reach, rank, target, steps


def lookup(table, index, size):
    choice = index[..., None] == jnp.arange(size, dtype=jnp.int32)
    return jnp.sum(jnp.where(choice, table, 0), axis=-1)


def plan_streams(arrived, reach, rank, target, route_ids, steps, capacity):
    ep = lax.axis_size("ep")
    me = lax.axis_index("ep")
    rows = CHUNKS * CHUNK
    tokens = rank.shape[1]
    codes = arrived[:, :capacity].astype(jnp.int32) - 1
    counts = arrived[:, 2 * capacity : 2 * capacity + 2 * steps].astype(jnp.int32)
    counts = counts.reshape(ep, 2, steps).transpose(1, 2, 0)
    counts = jnp.stack([counts[0], counts[1, :, ::-1]])
    start = jnp.zeros((2, ep), jnp.int32)
    starts, lives = [start], [counts[:, 0]]
    for distance in range(1, steps):
        start = jnp.maximum(
            start + lives[-1], jnp.roll(start, 1, axis=1) + LAG * CHUNK
        )
        starts.append(start)
        lives.append(jnp.roll(counts[:, distance], distance, axis=1))
    starts = jnp.stack(starts, axis=1)
    lives = jnp.stack(lives, axis=1)
    fits = jnp.max(jnp.where(lives > 0, starts + lives, 0)) <= rows

    spot = jnp.stack([me, ep - 1 - me])
    column = jnp.arange(ep, dtype=jnp.int32)

    def at_device(table, device):
        return jnp.sum(jnp.where(column[None, None, :] == device[:, None, None], table, 0), axis=2)

    previous = (spot + ep - 1) % ep
    out_start, out_live = at_device(starts, spot), at_device(lives, spot)
    in_start, in_live = at_device(starts, previous), at_device(lives, previous)
    way_base = (jnp.arange(2, dtype=jnp.int32) * rows)[:, None]
    place = jnp.arange(rows, dtype=jnp.int32)

    def locate(start, live):
        distance = (
            jnp.sum((place[None, :, None] >= start[:, None, :]).astype(jnp.int32), axis=2) - 1
        )
        choice = distance[:, :, None] == jnp.arange(steps, dtype=jnp.int32)
        within = place[None] - jnp.sum(jnp.where(choice, start[:, None, :], 0), axis=2)
        valid = within < jnp.sum(jnp.where(choice, live[:, None, :], 0), axis=2)
        return choice, within, valid

    own_list = jnp.sum(
        jnp.where(
            rank[:, None, :] == jnp.arange(tokens, dtype=jnp.int32)[None, :, None],
            jnp.arange(tokens, dtype=jnp.int32)[None, None, :],
            0,
        ),
        axis=2,
    )
    own_list = jnp.pad(own_list, ((0, 0), (0, rows - tokens)))
    zero_row = 2 * rows + tokens
    choice, within, valid = locate(out_start, out_live)
    shifted = jnp.concatenate([jnp.zeros((2, 1), jnp.int32), in_start[:, :-1]], axis=1)
    source = way_base + within + jnp.sum(jnp.where(choice, shifted[:, None, :], 0), axis=2)
    source = jnp.where(choice[:, :, 0], 2 * rows + own_list, source)
    pick = jnp.clip(jnp.where(valid, source, zero_row), 0, zero_row)

    none_row = 2 * rows
    choice, within, valid = locate(in_start, in_live)
    next_start = jnp.concatenate([out_start[:, 1:], jnp.zeros((2, 1), jnp.int32)], axis=1)
    next_live = jnp.concatenate([out_live[:, 1:], jnp.zeros((2, 1), jnp.int32)], axis=1)
    goes_on = valid & (within < jnp.sum(jnp.where(choice, next_live[:, None, :], 0), axis=2))
    onward = way_base + within + jnp.sum(jnp.where(choice, next_start[:, None, :], 0), axis=2)
    onward = jnp.clip(jnp.where(goes_on, onward, none_row), 0, none_row)

    source_of = jnp.arange(ep, dtype=jnp.int32)
    far = jnp.stack([(me - 1 - source_of) % ep, (source_of - me - 1) % ep])
    base = jnp.stack([lookup(in_start[way], far[way], steps) for way in (0, 1)])
    way_of = (codes >= tokens).astype(jnp.int32)
    spot_of = jnp.where(
        way_of == 1, rows + base[1][:, None] + codes - tokens, base[0][:, None] + codes
    )
    spot_of = jnp.where(codes >= 2 * tokens, 2 * rows + codes - 2 * tokens, spot_of)
    expert = jnp.clip(jnp.where(codes >= 0, spot_of, zero_row), 0, zero_row).reshape(-1)

    total = ep * capacity
    index = jnp.arange(total, dtype=jnp.int32)
    result_pick = jnp.sum(
        jnp.where(
            (way_base + place[None])[:, :, None] == expert[None, None, :],
            index[None, None, :] - total,
            0,
        ),
        axis=2,
    ) + total

    back = jnp.where(reach > 0, way_base + rank, none_row)
    mine = route_ids == me
    local = jnp.sum(jnp.where(mine, target - total, 0), axis=1) + total
    final = jnp.concatenate([jnp.clip(back, 0, none_row), local[None]], axis=0)
    return fits, pick, expert, result_pick, onward, final


def feed_forward(rows, full_gate, full_up, full_down):
    gate_pre = jnp.dot(rows, full_gate, preferred_element_type=jnp.float32)
    up_pre = jnp.dot(rows, full_up, preferred_element_type=jnp.float32)
    hidden = (jax.nn.silu(gate_pre) * up_pre).astype(jnp.bfloat16)
    return jnp.dot(hidden, full_down, preferred_element_type=jnp.float32).astype(jnp.bfloat16)


def padded_exchange(normed, target, route_weights, weights, ep_size, capacity):
    row_count, features = normed.shape
    outbound = jnp.zeros((ep_size * capacity, features), jnp.bfloat16)
    for column in range(target.shape[1]):
        outbound = outbound.at[target[:, column]].set(normed)
    outbound = outbound.reshape(ep_size, capacity, features)
    arrived = lax.all_to_all(outbound, "ep", split_axis=0, concat_axis=0, tiled=True)
    result = feed_forward(arrived.reshape(-1, features), *weights)
    returned_rows = send_back(result.reshape(ep_size, capacity, features))
    returned_rows = returned_rows.reshape(ep_size * capacity, features)
    combined = jnp.zeros((row_count, features), jnp.float32)
    for column in range(target.shape[1]):
        picked = returned_rows[target[:, column]].astype(jnp.float32)
        combined = combined + route_weights[:, column : column + 1] * picked
    return combined.astype(jnp.bfloat16)


def per_device(
    tokens, norm_gain, route_ids, route_weights, w_gate, w_up, w_down, dispatch=dispatch, collect=collect
):
    row_count, features = tokens.shape
    ep_size = lax.axis_size("ep")
    capacity = row_count * GROUPS // ep_size
    floats = tokens.astype(jnp.float32)
    inverse = lax.rsqrt(jnp.mean(floats * floats, axis=1, keepdims=True) + epsilon)
    normed = (floats * inverse * norm_gain).astype(jnp.bfloat16)
    weights = (
        lax.all_gather(w_gate, "tp", axis=2, tiled=True)[0],
        lax.all_gather(w_up, "tp", axis=2, tiled=True)[0],
        lax.all_gather(w_down, "tp", axis=1, tiled=True)[0],
    )
    message, reach, rank, target, steps = plan_routes(route_ids, route_weights, capacity)
    arrived = lax.all_to_all(message, "ep", split_axis=0, concat_axis=0, tiled=True)
    fits, pick, expert, result_pick, onward, final = plan_streams(
        arrived, reach, rank, target, route_ids, steps, capacity
    )
    expert_rows = dispatch(pick, expert, normed.reshape(row_count, -1, LANES))
    result = feed_forward(expert_rows.reshape(-1, features), *weights)
    scale = arrived[:, capacity : 2 * capacity].reshape(-1, 1)
    result = (result.astype(jnp.float32) * scale).astype(jnp.bfloat16)
    result = jnp.pad(result.reshape(-1, features // LANES, LANES), ((0, 1), (0, 0), (0, 0)))
    mixed = collect(result_pick, onward, final, result).reshape(row_count, features)
    return lax.cond(
        fits,
        lambda: mixed,
        lambda: padded_exchange(normed, target, route_weights, weights, ep_size, capacity),
    )


def solution(mesh):
    in_specs = (
        P(("grp", "ep", "tp"), None),
        P(),
        P(("grp", "ep", "tp"), None),
        P(("grp", "ep", "tp"), None),
        P("ep", None, "tp"),
        P("ep", None, "tp"),
        P("ep", "tp", None),
    )
    out_specs = P(("grp", "ep", "tp"), None)
    return jax.shard_map(
        per_device, mesh=mesh, in_specs=in_specs, out_specs=out_specs, check_vma=False
    )
```

time: 849 us -> 509 us (0.60); the launches traced: 836 us -> 509 us
  waiting for transfers between devices: 723 us -> 19.8 us
  Pallas kernels: 0 us -> 399 us
  starting transfers between devices: 55 us -> 32.8 us
    all_to_all x2 -> x1, waiting for transfers between devices: 693 us -> 17.6 us  [per_device(): lax.all_to_all(message, 'ep', split_axis=0, concat_axis=0, tiled=True)]
    pallas_call x0 -> x2, Pallas kernels: none -> 399 us  [ring_call(): pl.pallas_call(kernel, out_shape=jax.ShapeDtypeStruct((out_rows,) + row_s...]
    all_gather x3, waiting for transfers between devices: 28 us -> 0.04 us  [the longest x1 0.02 us: per_device(): lax.all_gather(w_up, 'tp', axis=2, tiled=True)[0]]
    all_to_all x2 -> x1, starting transfers between devices: 54.6 us -> 32.7 us  [per_device(): lax.all_to_all(message, 'ep', split_axis=0, concat_axis=0, tiled=True)]
    scatter x2 -> x0, other arithmetic: 12.1 us -> none  [per_device(): outbound = outbound.at[target[:, column]].set(normed)]
    gather x2 -> x0, local copies, waits for them, and re-layouts: 10.2 us -> none  [per_device(): picked = returned_rows[target[:, column]].astype(jnp.float32)]
  transfers between devices with their start and end apart: 5 -> 4, of which waited for: 3 -> 1; matrix products, arithmetic and copies ran while one was open for 1% -> 5% of each run, Pallas kernels for 0% -> 40%
where the time goes in v1:
time: 509 us
  Pallas kernels  399 us (78%)
  starting transfers between devices  32.8 us (6%)
  waiting for transfers between devices  19.8 us (4%)
  matrix products  15.2 us (3%)
  local copies, waits for them, and re-layouts  14.6 us (3%)
  between operations  14.2 us (3%)
  other arithmetic  12.7 us (2%)
    pallas_call x2, Pallas kernels, ring_call(): pl.pallas_call(kernel, out_shape=jax.ShapeDtypeStruct((out_rows,) + row_s...  399 us
    all_to_all x1, starting transfers between devices, per_device(): lax.all_to_all(message, 'ep', split_axis=0, concat_axis=0, tiled=True)  32.7 us
    all_to_all x1, waiting for transfers between devices, per_device(): lax.all_to_all(message, 'ep', split_axis=0, concat_axis=0, tiled=True)  17.6 us
  transfers between devices with their start and end apart: 4, of which 1 were waited for; matrix products, arithmetic and copies ran while one was open for 5% of the time, Pallas kernels for 40%

profile of v1, /device:TPU:46, one launch (start us, length us, event | category | flops | bytes accessed | tf_op | source)
XLA Modules:
  0.0 508.8 jit_solution(11421435689003076607)
XLA Ops:
  6.6 0.7 all-gather.4.cloned.1.call-update
  7.4 0.7 all-gather.6.cloned.1.call-update
  8.2 0.3 convert_reduce_fusion.1
  8.7 0.3 convert_reduce_fusion
  9.0 0.7 select_reduce_fusion.3
  9.9 0.1 convert_reduce_fusion.3
  10.3 0.6 pad.16
  10.9 32.7 %all-to-all-start.2 = ((f32[32,1,128]{2,1,0:T(1,128)}), f32[32,1,128]{2,1,0:T(1,128)S(1)}, u32[]{:S(2)}, u32[]{:S(2)}) async-start(f32[32,1,128]{2,1,0:T(1,128)} %bitcast.22), calls=%async_computation.2 | async-start | bytes 32768 | tf_op jit(solution)/shard_map/all_to_all | solution.py:410
  43.6 0.7 all-gather.8.cloned.1.call-update
  44.4 0.3 fusion.10
  44.7 0.3 fusion.151
  45.1 0.3 fusion.12
  45.6 0.6 pad_add_fusion.final_ref
  46.2 1.2 copy.515
  47.4 0.1 select_reduce_fusion.5
  47.6 17.6 %all-to-all-done.2 = f32[32,1,128]{2,1,0:T(1,128)S(1)} async-done(((f32[32,1,128]{2,1,0:T(1,128)}), f32[32,1,128]{2,1,0:T(1,128)S(1)}, u32[]{:S(2)}, u32[]{:S(2)}) %all-to-all-start.2) | async-done | bytes 16416 | tf_op jit(solution)/shard_map/all_to_all | solution.py:410
  65.2 0.1 copy.390
  70.6 0.1 stack.140
  70.7 0.2 fusion.103
  70.9 0.1 stack.141
  71.0 0.8 select_reduce_fusion.13
  71.9 0.1 copy.507
  72.0 0.1 copy.508
  72.1 0.1 copy.503
  72.2 0.3 fusion.18
  72.5 0.1 copy.511
  72.6 0.1 copy.512
  72.7 0.1 copy.504
  72.8 0.3 fusion.19
  73.2 0.1 copy.513
  73.3 0.2 iota_compare_fusion.3
  73.5 0.1 select_reduce_fusion.19
  73.6 0.1 select_reduce_fusion.18
  73.7 0.9 select_reduce_fusion.12
  74.6 0.6 select_reduce_fusion.8
  75.3 0.7 eq.247.expert_ref
  76.8 0.7 fusion.22
  77.5 201.3 %dispatch.1 = bf16[1024,16,128]{2,1,0:T(8,128)(2,1)} custom-call(s32[2,2048]{1,0:T(2,128)} %get-tuple-element.172.pick_ref, s32[1024]{0:T(1024)} %eq.247.expert_ref, bf16[256,16,128]{2,1,0:T(8,128)(2,1)} %bitcast.439), custom_call_target="tpu_custom_call" | custom-call | tf_op jit(solution)/shard_map/dispatch/pallas_call | solution.py:166
  278.8 2.3 select_reduce_fusion
  281.1 0.6 broadcast_add_fusion.2.result_ref
  281.7 5.2 %fusion.6 = f32[1024,512]{1,0:T(8,128)S(1)} fusion(bf16[128,8,16,128]{3,2,1,0:T(8,128)(2,1)} %bitcast.434, bf16[1,2048,512]{2,1,0:T(8,128)(2,1)} %all-gather.4.cloned.1.call-done), kind=kOutput, calls=%fused_computation.20 | convolution fusion | flops 2147483648 | bytes 8388608 | tf_op jit(solution)/shard_map/dot_general | solution.py:372
  287.0 10.0 %fusion.3 = bf16[128,8,16,128]{3,1,2,0:T(8,128)(2,1)} fusion(f32[1024]{0:T(1024)S(1)} %mul.91, f32[1024,512]{1,0:T(8,128)S(1)} %fusion.6, bf16[128,8,16,128]{3,2,1,0:T(8,128)(2,1)} %bitcast.435, bf16[1,512,2048]{2,1,0:T(8,128)(2,1)} %all-gather.8.cloned.1.call-done, bf16[1,2048,512]{2,1,0:T(8,128)(2,1)} %all-gather.6.cloned.1.call-done), kind=kOutput, calls=%fused_computation.17 | convolution fusion | flops 4306501632 | bytes 14684160 | tf_op jit(solution)/shard_map/dot_general | solution.py:375
  297.0 3.6 copy.517
  300.6 2.3 pad.18.result
  302.9 197.9 %collect.1 = bf16[256,16,128]{2,1,0:T(8,128)(2,1)S(1)} custom-call(s32[2,2048]{1,0:T(2,128)} %broadcast_add_fusion.2.result_ref, s32[2,2048]{1,0:T(2,128)} %get-tuple-element.173.onward_ref, s32[3,256]{1,0:T(4,128)} %pad_add_fusion.final_ref, bf16[1025,16,128]{2,1,0:T(8,128)(2,1)} %pad.18.result), custom_call_target="tpu_custom_call" | custom-call | tf_op jit(solution)/shard_map/collect/pallas_call | solution.py:166
  500.8 0.6 conditional.1
  501.1 0.3 copy.531
  501.3 1.0 copy-done.2
  (136 shorter events, 6.7 us)
Async XLA Ops:
  6.5 1.6 copy-start.4
  6.5 2.5 copy-start.6
  6.6 37.9 %copy-start = (bf16[256,2048]{1,0:T(8,128)(2,1)S(1)}, bf16[256,2048]{1,0:T(8,128)(2,1)}, u32[]{:S(2)}) copy-start(bf16[256,2048]{1,0:T(8,128)(2,1)} %param.9) | copy-start | bytes 3145732
  6.6 275.1 %all-gather.4.cloned.1.call-start = ((), (), s32[]{:S(2)}) async-start(), calls=%async_computation.3 | async-start | bytes 3145728 | tf_op jit(solution)/shard_map/all_gather | solution.py:405
  7.3 37.4 %copy-start.3 = (f32[2048]{0:T(1024)S(1)}, f32[2048]{0:T(1024)}, u32[]{:S(2)}) copy-start(f32[2048]{0:T(1024)} %param.10) | copy-start | bytes 24580
  7.3 279.6 %all-gather.6.cloned.1.call-start = ((), (), s32[]{:S(2)}) async-start(), calls=%async_computation.4 | async-start | bytes 3145728 | tf_op jit(solution)/shard_map/all_gather | solution.py:406
  10.9 54.3 %all-to-all-start.2 = ((f32[32,1,128]{2,1,0:T(1,128)}), f32[32,1,128]{2,1,0:T(1,128)S(1)}, u32[]{:S(2)}, u32[]{:S(2)}) async-start(f32[32,1,128]{2,1,0:T(1,128)} %bitcast.22), calls=%async_computation.2 | async-start | bytes 32768 | tf_op jit(solution)/shard_map/all_to_all | solution.py:410
  43.6 243.4 %all-gather.8.cloned.1.call-start = ((), (), s32[]{:S(2)}) async-start(), calls=%async_computation.5 | async-start | bytes 3145728 | tf_op jit(solution)/shard_map/all_gather | solution.py:407
  77.5 201.3 %copy-start.5 = (s32[1024]{0:T(1024)S(1)}, s32[1024]{0:T(1024)}, u32[]{:S(2)}) copy-start(s32[1024]{0:T(1024)} %eq.247.expert_ref) | copy-start | bytes 12292
  501.3 1.0 copy-start.2
Sparse Core Ops, SparseCore 0:
  9.2 38.3 all-gather.3
  49.3 28.4 all-gather.5
  79.7 28.7 all-gather.7
